TPU v7x, 32 devices: a whole 2x2x4 slice. The times are simulated.
32 devices in a mesh: ep: 16 (over z, y, x), tp: 2 (over core).
Axes of the slice: x: 2, y: 2, z: 4, core: 2. Of those that a mesh axis runs over, the one named last changes fastest.
Arguments:
- tokens: bfloat16 [512, 2048], P('ep'), may hold values from -6 to 6
- mix_gain: float32 [2048], replicated, may hold values from 0.1 to 1.9
- w_query: bfloat16 [2048, 512], P('ep', 'tp'), may hold values from -0.125 to 0.125
- w_key: bfloat16 [2048, 512], P('ep', 'tp'), may hold values from -0.125 to 0.125
- w_value: bfloat16 [2048, 512], P('ep', 'tp'), may hold values from -0.125 to 0.125
- w_outgate: bfloat16 [2048, 512], P('ep', 'tp'), may hold values from -0.125 to 0.125
- w_igate: bfloat16 [2048, 8], P('ep', 'tp'), may hold values from -0.125 to 0.125
- w_fgate: bfloat16 [2048, 8], P('ep', 'tp'), may hold values from -0.125 to 0.125
- igate_bias: float32 [8], P('tp'), may hold values from -2 to 1
- fgate_bias: float32 [8], P('tp'), may hold values from 0 to 4
- head_gain: float32 [512], P('tp'), may hold values from 0.1 to 1.9
- w_out: bfloat16 [512, 2048], P('tp', 'ep'), may hold values from -0.25 to 0.25
- state_matrix: float32 [512, 8, 64, 64], P('ep', 'tp'), may hold values from -2.4 to 2.4
- state_norm: float32 [512, 8, 64], P('ep', 'tp'), may hold values from -2.4 to 2.4
- state_max: float32 [512, 8], P('ep', 'tp'), may hold values from -4 to 4
- ffn_gain: float32 [2048], replicated, may hold values from 0.1 to 1.9
- w_expert_gate: bfloat16 [16, 2048, 1408], P('ep', None, 'tp'), may hold values from -0.125 to 0.125
- w_expert_up: bfloat16 [16, 2048, 1408], P('ep', None, 'tp'), may hold values from -0.125 to 0.125
- w_expert_down: bfloat16 [16, 1408, 2048], P('ep', 'tp'), may hold values from -0.15625 to 0.15625
- routes: int32 [512, 3], P('ep'), may hold values from 0 to 15, all different within a row; in each aligned block of 32 rows (0 to 31, 32 to 63, ...) at most 12 rows name the same one
- route_weights: float32 [512, 3], P('ep'), may hold values from 0.2 to 1
Outputs:
- mixed: bfloat16 [512, 2048], P('ep')
- new_matrix: float32 [512, 8, 64, 64], P('ep', 'tp')
- new_norm: float32 [512, 8, 64], P('ep', 'tp')
- new_max: float32 [512, 8], P('ep', 'tp')
Inputs may be any that keep to these rules, and one draw needn't show every extreme that they name: `routes`: each row names 3 different experts. Among the rows of one device, no expert is named by more than 12 rows, a bound that some block reaches.
All inputs are finite; a program needn't handle non-finite values.
Results may differ from a plain program's by a relative error of at most 0.017.
Values may be sent and summed in bfloat16 or wider, within the bound.
No kernel may reach another device: no remote copies, remote signals or barrier semaphores. Data moves between devices by JAX's collectives and lax.ppermute only.
A program may use at most 128 MiB of HBM per device.

v0:
```python
import jax
import jax.numpy as jnp
from jax import lax
from jax.sharding import PartitionSpec as P


def rms_scale(values_in, gain_vec):
    widened = values_in.astype(jnp.float32)
    return (
        widened * lax.rsqrt(jnp.mean(widened * widened, axis=-1, keepdims=True) + 1e-06) * gain_vec
    )


def memory_cell(
    query,
    key_row,
    value_row,
    outgate,
    input_pre,
    forget_pre,
    head_gain,
    state_matrix,
    state_norm,
    state_max,
):
    seq_rows, head_count = input_pre.shape
    head_size = query.shape[1] // head_count
    query_heads = query.astype(jnp.float32).reshape(seq_rows, head_count, head_size)
    key_heads = key_row.astype(jnp.float32).reshape(
        seq_rows, head_count, head_size
    ) * head_size ** (-0.5)
    value_heads = value_row.astype(jnp.float32).reshape(seq_rows, head_count, head_size)
    log_forget = jax.nn.log_sigmoid(forget_pre)
    new_max = jnp.maximum(log_forget + state_max, input_pre)
    keep_old = jnp.exp(log_forget + state_max - new_max)
    keep_new = jnp.exp(input_pre - new_max)
    new_matrix = (
        keep_old[:, :, None, None] * state_matrix
        + keep_new[:, :, None, None] * value_heads[:, :, :, None] * key_heads[:, :, None, :]
    )
    new_norm = keep_old[:, :, None] * state_norm + keep_new[:, :, None] * key_heads
    numerator = jnp.einsum(
        "bhvd,bhd->bhv", new_matrix, query_heads, precision=lax.Precision.HIGHEST
    )
    denominator = jnp.sum(new_norm * query_heads, axis=-1)
    cell_read = numerator / jnp.maximum(jnp.abs(denominator), jnp.exp(-new_max))[:, :, None]
    centered = cell_read - jnp.mean(cell_read, axis=-1, keepdims=True)
    variance = jnp.mean(centered * centered, axis=-1, keepdims=True)
    scaled_cell = (centered * lax.rsqrt(variance + 1e-06)).reshape(seq_rows, head_count * head_size)
    cell_out = (scaled_cell * head_gain * jax.nn.sigmoid(outgate.astype(jnp.float32))).astype(
        jnp.bfloat16
    )
    return (cell_out, new_matrix, new_norm, new_max)


def body(
    tokens,
    mix_gain,
    w_query,
    w_key,
    w_value,
    w_outgate,
    w_igate,
    w_fgate,
    igate_bias,
    fgate_bias,
    head_gain,
    w_out,
    state_matrix,
    state_norm,
    state_max,
    ffn_gain,
    w_expert_gate,
    w_expert_up,
    w_expert_down,
    routes,
    route_weights,
):
    seq_rows, width = tokens.shape
    normed = rms_scale(tokens, mix_gain).astype(jnp.bfloat16)
    weight_list = (w_query, w_key, w_value, w_outgate, w_igate, w_fgate)
    spread = lax.all_to_all(normed, "ep", split_axis=1, concat_axis=0, tiled=True)
    joined = jnp.concatenate(weight_list, axis=1)
    summed = lax.psum_scatter(
        jnp.dot(spread, joined, preferred_element_type=jnp.float32),
        "ep",
        scatter_dimension=0,
        tiled=True,
    )
    bounds = [0]
    for weight in weight_list:
        bounds.append(bounds[-1] + weight.shape[1])
    projected = tuple(
        (summed[:, bounds[index] : bounds[index + 1]] for index in range(len(weight_list)))
    )
    query = projected[0].astype(jnp.bfloat16)
    key_row = projected[1].astype(jnp.bfloat16)
    value_row = projected[2].astype(jnp.bfloat16)
    outgate = projected[3].astype(jnp.bfloat16)
    input_pre = projected[4] + igate_bias
    forget_pre = projected[5] + fgate_bias
    cell_out, new_matrix, new_norm, new_max = memory_cell(
        query,
        key_row,
        value_row,
        outgate,
        input_pre,
        forget_pre,
        head_gain,
        state_matrix,
        state_norm,
        state_max,
    )
    partial_out = jnp.dot(
        cell_out,
        lax.all_gather(w_out, "ep", axis=1, tiled=True),
        preferred_element_type=jnp.float32,
    )
    attended = lax.psum(partial_out.astype(jnp.bfloat16), "tp").astype(jnp.float32)
    resid = (tokens.astype(jnp.float32) + attended).astype(jnp.bfloat16)
    normed_two = rms_scale(resid, ffn_gain).astype(jnp.bfloat16)
    ep_count = lax.axis_size("ep")
    local_experts = w_expert_gate.shape[0]
    expert_total = local_experts * ep_count
    top_count = routes.shape[1]
    capacity = max(2, 2 * seq_rows * top_count // expert_total)
    flat_routes = routes.reshape(-1)
    onehot = (flat_routes[:, None] == jnp.arange(expert_total, dtype=jnp.int32)[None, :]).astype(
        jnp.int32
    )
    earlier = jnp.cumsum(onehot, axis=0, dtype=jnp.int32) - onehot
    slots = jnp.sum(onehot * earlier, axis=1, dtype=jnp.int32)
    targets = flat_routes * capacity + slots
    dispatch = (
        targets[:, None] == jnp.arange(expert_total * capacity, dtype=jnp.int32)[None, :]
    ).astype(jnp.bfloat16)
    route_rows = jnp.repeat(normed_two, top_count, axis=0)
    outgoing = jnp.einsum(
        "rs,rd->sd", dispatch, route_rows, preferred_element_type=jnp.float32
    ).astype(jnp.bfloat16)
    outgoing = outgoing.reshape(expert_total, capacity, width)
    received = lax.all_to_all(outgoing, "ep", split_axis=0, concat_axis=0, tiled=True)
    slot_count = received.shape[1]
    regrouped = received.reshape(ep_count, local_experts, slot_count, width)
    gate_pre = jnp.einsum(
        "nxcd,xdf->nxcf", regrouped, w_expert_gate, preferred_element_type=jnp.float32
    )
    up_pre = jnp.einsum(
        "nxcd,xdf->nxcf", regrouped, w_expert_up, preferred_element_type=jnp.float32
    )
    hidden = (jax.nn.silu(gate_pre) * up_pre).astype(jnp.bfloat16)
    partial_down = jnp.einsum(
        "nxcf,xfd->nxcd", hidden, w_expert_down, preferred_element_type=jnp.float32
    )
    expert_sum = lax.psum(partial_down.astype(jnp.bfloat16), "tp")
    finished = expert_sum.reshape(ep_count * local_experts, slot_count, width)
    returned = lax.all_to_all(finished, "ep", split_axis=0, concat_axis=0, tiled=True)
    picked = jnp.dot(
        dispatch,
        returned.reshape(expert_total * capacity, width),
        preferred_element_type=jnp.float32,
    )
    weighted = jnp.sum(
        picked.reshape(seq_rows, top_count, width) * route_weights[:, :, None], axis=1
    )
    mixed = (resid.astype(jnp.float32) + weighted).astype(jnp.bfloat16)
    return (mixed, new_matrix, new_norm, new_max)


def solution(mesh):
    placed = (
        P("ep", None),
        P(),
        P("ep", "tp"),
        P("ep", "tp"),
        P("ep", "tp"),
        P("ep", "tp"),
        P("ep", "tp"),
        P("ep", "tp"),
        P("tp"),
        P("tp"),
        P("tp"),
        P("tp", "ep"),
        P("ep", "tp", None, None),
        P("ep", "tp", None),
        P("ep", "tp"),
        P(),
        P("ep", None, "tp"),
        P("ep", None, "tp"),
        P("ep", "tp", None),
        P("ep", None),
        P("ep", None),
    )
    return jax.shard_map(
        body,
        mesh=mesh,
        in_specs=placed,
        out_specs=(P("ep", None), P("ep", "tp", None, None), P("ep", "tp", None), P("ep", "tp")),
        check_vma=False,
    )
```

profile of v0, /device:TPU:8, one launch (start us, length us, event | category | flops | bytes accessed | tf_op | source)
XLA Modules:
  0.0 342.0 jit_solution(8380659892496630698)
XLA Ops:
  7.2 0.0 copy-start
  7.2 1.2 fusion.36
  8.4 1.7 copy_bitcast_fusion
  10.1 7.2 %all-to-all-start = ((bf16[32,16,128]{2,0,1:T(8,128)(2,1)}), bf16[32,16,128]{2,0,1:T(8,128)(2,1)S(1)}, u32[]{:S(2)}, u32[]{:S(2)}) async-start(bf16[32,16,128]{2,0,1:T(8,128)(2,1)} %copy_bitcast_fusion), calls=%async_computation | async-start | bytes 262144 | tf_op jit(solution)/shard_map/all_to_all | solution.py:82
  17.3 0.0 reduce-scatter.2.cloned.1.call-start
  17.3 0.8 copy.58
  18.1 0.8 copy.59
  19.0 1.1 concatenate.3
  20.0 3.9 %all-to-all-done = bf16[32,16,128]{2,0,1:T(8,128)(2,1)S(1)} async-done(((bf16[32,16,128]{2,0,1:T(8,128)(2,1)}), bf16[32,16,128]{2,0,1:T(8,128)(2,1)S(1)}, u32[]{:S(2)}, u32[]{:S(2)}) %all-to-all-start) | async-done | bytes 131104 | tf_op jit(solution)/shard_map/all_to_all | solution.py:82
  23.9 1.9 fusion.62
  25.8 0.0 reduce-scatter.2.cloned.1.call-update
  25.8 0.0 all-gather.2.cloned.1.call-start
  25.8 0.7 all-gather.2.cloned.1.call-update
  26.5 0.0 all-reduce.3.cloned.1.call-start
  26.6 0.1 copy.60
  26.7 0.1 copy.61
  26.8 0.1 eq.50
  26.9 0.1 fusion.49
  27.0 0.1 reduce_window_sum.11
  27.1 0.2 select_reduce_fusion
  27.3 125.7 %reduce-scatter.2.cloned.1.call-done = f32[32,1032]{1,0:T(8,128)} async-done(((f32[512,1032]{1,0:T(8,128)}), f32[32,1032]{1,0:T(8,128)}) %reduce-scatter.2.cloned.1.call-update) | async-done | bytes 132112 | tf_op jit(solution)/shard_map/reduce_scatter | solution.py:84
  153.0 0.9 convert.9
  154.0 0.1 reshape.150
  154.1 0.1 reshape.171
  154.1 0.1 reshape.163
  154.2 0.1 reshape.161
  154.4 0.9 broadcast_multiply_fusion.3
  155.3 0.8 subtract_exponential_fusion.1
  156.1 0.8 multiply_reduce_fusion.1
  156.9 3.8 %multiply_add_fusion = f32[32,4,64,64]{3,2,1,0:T(8,128)S(1)} fusion(f32[32,4,64,64]{3,2,1,0:T(8,128)} %param.33, f32[32,4,64]{2,1,0:T(4,128)S(1)} %get-tuple-element.30, f32[32,4,64]{2,1,0:T(4,128)S(1)} %get-tuple-element.31, f32[32,4]{1,0:T(8,128)S(1)} %subtract_exponential_fusion.1), kind=kLoop, calls=%fused_computation | loop fusion | flops 1572864 | bytes 4260352 | tf_op jit(solution)/shard_map/add | solution.py:38
  160.7 0.0 copy-start.1
  160.7 2.0 copy-done.1
  162.7 3.4 fusion.63
  166.1 0.2 fusion.59
  166.3 0.2 multiply_reduce_fusion
  166.5 0.1 subtract_multiply_fusion
  166.6 0.1 reshape.152
  166.7 39.0 %all-gather.2.cloned.1.call-done = bf16[256,2048]{1,0:T(8,128)(2,1)} async-done(((bf16[256,128]{1,0:T(8,128)(2,1)}), bf16[256,2048]{1,0:T(8,128)(2,1)}) %all-gather.2.cloned.1.call-update) | async-done | bytes 1048592 | tf_op jit(solution)/shard_map/all_gather | solution.py:116
  205.7 2.2 convolution_convert_fusion.1
  207.8 0.0 all-reduce.3.cloned.1.call-update
  207.9 0.0 all-reduce.5.cloned.1.call-start
  207.9 0.5 multiply_add_fusion.3
  208.4 18.1 %all-reduce.3.cloned.1.call-done = bf16[32,2048]{1,0:T(8,128)(2,1)} async-done(((bf16[32,2048]{1,0:T(8,128)(2,1)}), bf16[32,2048]{1,0:T(8,128)(2,1)}) %all-reduce.3.cloned.1.call-update) | async-done | bytes 131088 | tf_op jit(solution)/shard_map/psum | solution.py:119
  226.5 1.1 fusion.40
  227.6 1.0 fusion.42
  228.6 0.2 broadcast_in_dim.2
  228.8 1.1 reshape.153
  229.9 2.4 convolution_convert_fusion
  232.3 2.1 reshape.154
  234.4 33.1 %all_to_all.29 = bf16[16,12,2048]{2,1,0:T(8,128)(2,1)S(1)} all-to-all(bf16[16,12,2048]{2,1,0:T(8,128)(2,1)} %reshape.154), channel_id=1, replica_groups=mesh['ep'=16,'tp'=2] {'ep'}, dimensions={0} | all-to-all | bytes 1572864 | tf_op jit(solution)/shard_map/all_to_all | solution.py:142
  267.5 1.0 copy-done.4
  268.5 3.8 %fusion.9 = f32[16,1,12,704]{3,0,2,1:T(8,128)} fusion(bf16[1,2048,704]{1,2,0:T(8,128)(2,1)} %param.37, bf16[16,12,2048]{2,1,0:T(8,128)(2,1)S(1)} %all_to_all.29), kind=kOutput, calls=%fused_computation.11 | convolution fusion | flops 553648128 | bytes 4210688 | tf_op jit(solution)/shard_map/nxcd,xdf->nxcf/dot_general | solution.py:145
  272.3 5.2 %fusion.6 = bf16[16,12,2048]{2,0,1:T(8,128)(2,1)} fusion(bf16[1,704,2048]{2,1,0:T(8,128)(2,1)S(1)} %copy-done, bf16[1,2048,704]{1,2,0:T(8,128)(2,1)} %param.38, f32[16,1,12,704]{3,0,2,1:T(8,128)} %fusion.9, bf16[16,12,2048]{2,1,0:T(8,128)(2,1)} %copy-done.4), kind=kOutput, calls=%fused_computation.7 | convolution fusion | flops 1108500480 | bytes 7880704 | tf_op jit(solution)/shard_map/nxcf,xfd->nxcd/dot_general | solution.py:152
  277.5 0.0 all-reduce.5.cloned.1.call-update
  277.6 17.9 %all-reduce.5.cloned.1.call-done = bf16[16,12,2048]{2,0,1:T(8,128)(2,1)} async-done(((bf16[16,12,2048]{2,0,1:T(8,128)(2,1)}), bf16[16,12,2048]{2,0,1:T(8,128)(2,1)}) %all-reduce.5.cloned.1.call-update) | async-done | bytes 786448 | tf_op jit(solution)/shard_map/psum | solution.py:155
  295.5 2.6 copy.65
  298.1 7.1 %all-to-all-start.2 = ((bf16[16,12,2048]{2,1,0:T(8,128)(2,1)}), bf16[16,12,2048]{2,1,0:T(8,128)(2,1)}, u32[]{:S(2)}, u32[]{:S(2)}) async-start(bf16[16,12,2048]{2,1,0:T(8,128)(2,1)} %copy.65), calls=%async_computation.3 | async-start | bytes 2097152 | tf_op jit(solution)/shard_map/all_to_all | solution.py:157
  305.2 0.1 reduce_sum.70
  305.3 0.1 copy.62
  305.4 0.7 copy.66
  306.0 25.1 %all-to-all-done.2 = bf16[16,12,2048]{2,1,0:T(8,128)(2,1)} async-done(((bf16[16,12,2048]{2,1,0:T(8,128)(2,1)}), bf16[16,12,2048]{2,1,0:T(8,128)(2,1)}, u32[]{:S(2)}, u32[]{:S(2)}) %all-to-all-start.2) | async-done | bytes 786464 | tf_op jit(solution)/shard_map/all_to_all | solution.py:157
  331.1 2.1 reshape.169
  333.2 1.5 fusion.18
  334.7 0.7 fusion.43
  (35 shorter events, 0.1 us)
Async XLA Ops:
  7.2 265.2 %copy-start = (bf16[1,704,2048]{2,1,0:T(8,128)(2,1)S(1)}, bf16[1,704,2048]{2,1,0:T(8,128)(2,1)}, u32[]{:S(2)}) copy-start(bf16[1,704,2048]{2,1,0:T(8,128)(2,1)} %param.39) | copy-start | bytes 8650756
  10.1 13.8 %all-to-all-start = ((bf16[32,16,128]{2,0,1:T(8,128)(2,1)}), bf16[32,16,128]{2,0,1:T(8,128)(2,1)S(1)}, u32[]{:S(2)}, u32[]{:S(2)}) async-start(bf16[32,16,128]{2,0,1:T(8,128)(2,1)} %copy_bitcast_fusion), calls=%async_computation | async-start | bytes 262144 | tf_op jit(solution)/shard_map/all_to_all | solution.py:82
  17.3 135.7 %reduce-scatter.2.cloned.1.call-start = ((), (), s32[]{:S(2)}) async-start(), calls=%async_computation.4 | async-start | bytes 2506752 | tf_op jit(solution)/shard_map/reduce_scatter | solution.py:84
  18.9 7.6 %copy-start.13 = (f32[32,4]{0,1:T(4,128)S(1)}, f32[32,4]{0,1:T(4,128)}, u32[]{:S(2)}) copy-start(f32[32,4]{0,1:T(4,128)} %param.35) | copy-start | bytes 1540
  18.9 7.7 %copy-start.7 = (s32[32,3]{0,1:T(4,128)S(1)}, s32[32,3]{0,1:T(4,128)}, u32[]{:S(2)}) copy-start(s32[32,3]{0,1:T(4,128)} %param.40) | copy-start | bytes 1156
  23.9 130.5 %copy-start.10 = (f32[4]{0:T(128)S(1)}, f32[4]{0:T(128)}, u32[]{:S(2)}) copy-start(f32[4]{0:T(128)} %param.30) | copy-start | bytes 52
  23.9 130.5 %copy-start.15 = (f32[4]{0:T(128)S(1)}, f32[4]{0:T(128)}, u32[]{:S(2)}) copy-start(f32[4]{0:T(128)} %param.29) | copy-start | bytes 52
  23.9 132.2 %copy-start.5 = (f32[32,4,64]{2,1,0:T(4,128)S(1)}, f32[32,4,64]{2,1,0:T(4,128)}, u32[]{:S(2)}) copy-start(f32[32,4,64]{2,1,0:T(4,128)} %param.34) | copy-start | bytes 98308
  25.8 179.9 %all-gather.2.cloned.1.call-start = ((), (), s32[]{:S(2)}) async-start(), calls=%async_computation.5 | async-start | bytes 1114112 | tf_op jit(solution)/shard_map/all_gather | solution.py:116
  26.5 200.0 %all-reduce.3.cloned.1.call-start = ((), (), s32[]{:S(2)}) async-start(), calls=%async_computation.6 | async-start | bytes 262144 | tf_op jit(solution)/shard_map/psum | solution.py:119
  27.3 180.6 %copy-start.11 = (s32[96]{0:T(128)}, s32[96]{0:T(128)S(1)}, u32[]{:S(2)}) copy-start(s32[96]{0:T(128)S(1)} %select_reduce_fusion) | copy-start | bytes 1156
  160.7 2.0 copy-start.1
  162.7 43.0 %copy-start.14 = (f32[256]{0:T(256)S(1)}, f32[256]{0:T(256)}, u32[]{:S(2)}) copy-start(f32[256]{0:T(256)} %param.31) | copy-start | bytes 3076
  162.7 63.8 %copy-start.2 = (bf16[32,2048]{1,0:T(8,128)(2,1)S(1)}, bf16[32,2048]{1,0:T(8,128)(2,1)}, u32[]{:S(2)}) copy-start(bf16[32,2048]{1,0:T(8,128)(2,1)} %param.21) | copy-start | bytes 393220
  162.7 64.9 %copy-start.6 = (f32[2048]{0:T(1024)S(1)}, f32[2048]{0:T(1024)}, u32[]{:S(2)}) copy-start(f32[2048]{0:T(1024)} %param.36) | copy-start | bytes 24580
  207.9 87.6 %all-reduce.5.cloned.1.call-start = ((), (), s32[]{:S(2)}) async-start(), calls=%async_computation.7 | async-start | bytes 1572864 | tf_op jit(solution)/shard_map/psum | solution.py:155
  267.5 1.0 copy-start.4
  277.5 27.7 %copy-start.12 = (s32[96]{0:T(128)S(1)}, s32[96]{0:T(128)}, u32[]{:S(2)}) copy-start(s32[96]{0:T(128)} %copy-done.11) | copy-start | bytes 1156
  277.5 27.8 %copy-start.8 = (s32[32,3]{0,1:T(4,128)S(1)}, s32[32,3]{0,1:T(4,128)}, u32[]{:S(2)}) copy-start(s32[32,3]{0,1:T(4,128)} %param.40) | copy-start | bytes 1156
  277.6 55.7 %copy-start.9 = (f32[32,3]{0,1:T(4,128)S(1)}, f32[32,3]{0,1:T(4,128)}, u32[]{:S(2)}) copy-start(f32[32,3]{0,1:T(4,128)} %param.41) | copy-start | bytes 1156
  298.1 36.6 %copy-start.3 = (bf16[32,2048]{1,0:T(8,128)(2,1)S(1)}, bf16[32,2048]{1,0:T(8,128)(2,1)}, u32[]{:S(2)}) copy-start(bf16[32,2048]{1,0:T(8,128)(2,1)} %all-reduce.3.cloned.1.call-done) | copy-start | bytes 393220
  298.1 33.0 %all-to-all-start.2 = ((bf16[16,12,2048]{2,1,0:T(8,128)(2,1)}), bf16[16,12,2048]{2,1,0:T(8,128)(2,1)}, u32[]{:S(2)}, u32[]{:S(2)}) async-start(bf16[16,12,2048]{2,1,0:T(8,128)(2,1)} %copy.65), calls=%async_computation.3 | async-start | bytes 2097152 | tf_op jit(solution)/shard_map/all_to_all | solution.py:157
Sparse Core Ops, SparseCore 0:
  25.9 127.0 reduce-scatter.1
  155.7 49.9 all-gather.1
  208.6 17.9 all-reduce.2
  277.7 17.7 all-reduce.4
where the time goes:
time: 343 us; the launch traced here: 342 us
  waiting for transfers between devices  230 us (67%)
  blocking collectives  33.1 us (10%)
  matrix products  20.2 us (6%)
  local copies, waits for them, and re-layouts  15.4 us (4%)
  starting transfers between devices  14.5 us (4%)
  other arithmetic  14.3 us (4%)
  between operations  14 us (4%)
    reduce_scatter x1, waiting for transfers between devices, body(): lax.psum_scatter(jnp.dot(spread, joined, preferred_element_type=jnp.float...  126 us
    all_gather x1, waiting for transfers between devices, body(): lax.all_gather(w_out, 'ep', axis=1, tiled=True)  39 us
    all_to_all x1, blocking collectives, body(): lax.all_to_all(outgoing, 'ep', split_axis=0, concat_axis=0, tiled=True)  33.1 us
    all_to_all x1, waiting for transfers between devices, body(): lax.all_to_all(finished, 'ep', split_axis=0, concat_axis=0, tiled=True)  25.1 us
    psum x1, waiting for transfers between devices, body(): lax.psum(partial_out.astype(jnp.bfloat16), 'tp').astype(jnp.float32)  18.1 us
    psum x1, waiting for transfers between devices, body(): expert_sum = lax.psum(partial_down.astype(jnp.bfloat16), 'tp')  17.9 us
    all_to_all x1, starting transfers between devices, body(): lax.all_to_all(normed, 'ep', split_axis=1, concat_axis=0, tiled=True)  7.22 us
    all_to_all x1, starting transfers between devices, body(): lax.all_to_all(finished, 'ep', split_axis=0, concat_axis=0, tiled=True)  7.11 us
  transfers between devices with their start and end apart: 6, of which 6 were waited for; matrix products, arithmetic and copies ran while one was open for 5% of the time, Pallas kernels for 0%

commit v1 on v0

--- a/solution.py
+++ b/solution.py
@@ -152,7 +152,7 @@
     partial_down = jnp.einsum(
         "nxcf,xfd->nxcd", hidden, w_expert_down, preferred_element_type=jnp.float32
     )
-    expert_sum = lax.psum(partial_down.astype(jnp.bfloat16), "tp")
+    expert_sum = jnp.sum(lax.all_gather(partial_down.astype(jnp.bfloat16), "tp"), axis=0)
     finished = expert_sum.reshape(ep_count * local_experts, slot_count, width)
     returned = lax.all_to_all(finished, "ep", split_axis=0, concat_axis=0, tiled=True)
     picked = jnp.dot(

time: 343 us -> 337 us (0.983)
  waiting for transfers between devices: 230 us -> 221 us
    psum x1 -> x0, waiting for transfers between devices: 17.9 us -> none  [body(): expert_sum = lax.psum(partial_down.astype(jnp.bfloat16), 'tp')]
    all_gather x0 -> x1, waiting for transfers between devices: none -> 8.72 us  [body(): lax.all_gather(partial_down.astype(jnp.bfloat16), 'tp')]
where the time goes in v1:
time: 337 us; the launch traced here: 336 us
  waiting for transfers between devices  221 us (66%)
  blocking collectives  33.1 us (10%)
  matrix products  20.2 us (6%)
  other arithmetic  17.1 us (5%)
  local copies, waits for them, and re-layouts  15.5 us (5%)
  starting transfers between devices  14.5 us (4%)
  between operations  14 us (4%)
    reduce_scatter x1, waiting for transfers between devices, body(): lax.psum_scatter(jnp.dot(spread, joined, preferred_element_type=jnp.float...  126 us
    all_gather x1, waiting for transfers between devices, body(): lax.all_gather(w_out, 'ep', axis=1, tiled=True)  39 us
    all_to_all x1, blocking collectives, body(): lax.all_to_all(outgoing, 'ep', split_axis=0, concat_axis=0, tiled=True)  33.1 us
    all_to_all x1, waiting for transfers between devices, body(): lax.all_to_all(finished, 'ep', split_axis=0, concat_axis=0, tiled=True)  25.1 us
    psum x1, waiting for transfers between devices, body(): lax.psum(partial_out.astype(jnp.bfloat16), 'tp').astype(jnp.float32)  18.1 us
    all_gather x1, waiting for transfers between devices, body(): lax.all_gather(partial_down.astype(jnp.bfloat16), 'tp')  8.72 us
    all_to_all x1, starting transfers between devices, body(): lax.all_to_all(normed, 'ep', split_axis=1, concat_axis=0, tiled=True)  7.22 us
    all_to_all x1, starting transfers between devices, body(): lax.all_to_all(finished, 'ep', split_axis=0, concat_axis=0, tiled=True)  7.11 us
  transfers between devices with their start and end apart: 6, of which 6 were waited for; matrix products, arithmetic and copies ran while one was open for 5% of the time, Pallas kernels for 0%

profile of v1, /device:TPU:8, one launch (start us, length us, event | category | flops | bytes accessed | tf_op | source)
XLA Modules:
  0.0 335.7 jit_solution(10620202556017459230)
XLA Ops:
  7.2 0.0 copy-start
  7.2 1.2 fusion.37
  8.4 1.7 copy_bitcast_fusion
  10.1 7.2 %all-to-all-start = ((bf16[32,16,128]{2,0,1:T(8,128)(2,1)}), bf16[32,16,128]{2,0,1:T(8,128)(2,1)S(1)}, u32[]{:S(2)}, u32[]{:S(2)}) async-start(bf16[32,16,128]{2,0,1:T(8,128)(2,1)} %copy_bitcast_fusion), calls=%async_computation | async-start | bytes 262144 | tf_op jit(solution)/shard_map/all_to_all | solution.py:82
  17.3 0.0 reduce-scatter.2.cloned.1.call-start
  17.3 0.8 copy.69
  18.1 0.8 copy.70
  19.0 1.1 concatenate.3
  20.0 3.9 %all-to-all-done = bf16[32,16,128]{2,0,1:T(8,128)(2,1)S(1)} async-done(((bf16[32,16,128]{2,0,1:T(8,128)(2,1)}), bf16[32,16,128]{2,0,1:T(8,128)(2,1)S(1)}, u32[]{:S(2)}, u32[]{:S(2)}) %all-to-all-start) | async-done | bytes 131104 | tf_op jit(solution)/shard_map/all_to_all | solution.py:82
  23.9 1.9 fusion.63
  25.8 0.0 reduce-scatter.2.cloned.1.call-update
  25.8 0.0 all-gather.4.cloned.1.call-start
  25.8 0.7 all-gather.4.cloned.1.call-update
  26.5 0.0 all-reduce.2.cloned.1.call-start
  26.6 0.1 copy.71
  26.7 0.1 copy.72
  26.8 0.1 eq.50
  26.9 0.1 fusion.50
  27.0 0.1 reduce_window_sum.11
  27.1 0.2 select_reduce_fusion
  27.3 125.7 %reduce-scatter.2.cloned.1.call-done = f32[32,1032]{1,0:T(8,128)} async-done(((f32[512,1032]{1,0:T(8,128)}), f32[32,1032]{1,0:T(8,128)}) %reduce-scatter.2.cloned.1.call-update) | async-done | bytes 132112 | tf_op jit(solution)/shard_map/reduce_scatter | solution.py:84
  153.0 0.9 convert.10
  154.0 0.1 reshape.150
  154.1 0.1 reshape.172
  154.1 0.1 reshape.162
  154.2 0.1 reshape.160
  154.4 0.9 broadcast_multiply_fusion.3
  155.3 0.8 subtract_exponential_fusion.1
  156.1 0.8 multiply_reduce_fusion.1
  156.9 3.8 %multiply_add_fusion = f32[32,4,64,64]{3,2,1,0:T(8,128)S(1)} fusion(f32[32,4,64,64]{3,2,1,0:T(8,128)} %param.33, f32[32,4,64]{2,1,0:T(4,128)S(1)} %get-tuple-element.34, f32[32,4,64]{2,1,0:T(4,128)S(1)} %get-tuple-element.35, f32[32,4]{1,0:T(8,128)S(1)} %subtract_exponential_fusion.1), kind=kLoop, calls=%fused_computation | loop fusion | flops 1572864 | bytes 4260352 | tf_op jit(solution)/shard_map/add | solution.py:38
  160.7 2.0 copy-done.1
  162.7 3.4 fusion.64
  166.1 0.2 fusion.60
  166.3 0.2 multiply_reduce_fusion
  166.5 0.1 subtract_multiply_fusion
  166.6 0.1 reshape.152
  166.7 39.0 %all-gather.4.cloned.1.call-done = bf16[256,2048]{1,0:T(8,128)(2,1)} async-done(((bf16[256,128]{1,0:T(8,128)(2,1)}), bf16[256,2048]{1,0:T(8,128)(2,1)}) %all-gather.4.cloned.1.call-update) | async-done | bytes 1048592 | tf_op jit(solution)/shard_map/all_gather | solution.py:116
  205.7 2.2 convolution_convert_fusion.1
  207.8 0.0 all-reduce.2.cloned.1.call-update
  207.9 0.0 all-gather.6.cloned.1.call-start
  207.9 0.5 multiply_add_fusion.3
  208.4 18.1 %all-reduce.2.cloned.1.call-done = bf16[32,2048]{1,0:T(8,128)(2,1)} async-done(((bf16[32,2048]{1,0:T(8,128)(2,1)}), bf16[32,2048]{1,0:T(8,128)(2,1)}) %all-reduce.2.cloned.1.call-update) | async-done | bytes 131088 | tf_op jit(solution)/shard_map/psum | solution.py:119
  226.5 1.1 fusion.41
  227.6 1.0 fusion.43
  228.6 0.2 broadcast_in_dim.2
  228.8 1.1 reshape.153
  229.9 2.4 convolution_convert_fusion
  232.3 2.2 reshape.154
  234.5 33.1 %all_to_all.29 = bf16[16,12,2048]{2,1,0:T(8,128)(2,1)S(1)} all-to-all(bf16[16,12,2048]{2,1,0:T(8,128)(2,1)} %reshape.154), channel_id=1, replica_groups=mesh['ep'=16,'tp'=2] {'ep'}, dimensions={0} | all-to-all | bytes 1572864 | tf_op jit(solution)/shard_map/all_to_all | solution.py:142
  267.6 1.0 copy-done.4
  268.6 3.8 %fusion.12 = f32[16,1,12,704]{3,0,2,1:T(8,128)} fusion(bf16[1,2048,704]{1,2,0:T(8,128)(2,1)} %param.37, bf16[16,12,2048]{2,1,0:T(8,128)(2,1)S(1)} %all_to_all.29), kind=kOutput, calls=%fused_computation.12 | convolution fusion | flops 553648128 | bytes 4210688 | tf_op jit(solution)/shard_map/nxcd,xdf->nxcf/dot_general | solution.py:145
  272.4 5.2 %fusion.9 = bf16[16,1,12,2048]{3,0,2,1:T(8,128)(2,1)} fusion(bf16[1,704,2048]{2,1,0:T(8,128)(2,1)S(1)} %copy-done, bf16[1,2048,704]{1,2,0:T(8,128)(2,1)} %param.38, f32[16,1,12,704]{3,0,2,1:T(8,128)} %fusion.12, bf16[16,12,2048]{2,1,0:T(8,128)(2,1)} %copy-done.4), kind=kOutput, calls=%fused_computation.9 | convolution fusion | flops 1108500480 | bytes 7880704 | tf_op jit(solution)/shard_map/nxcf,xfd->nxcd/dot_general | solution.py:152
  277.6 0.0 all-gather.6.cloned.1.call-update
  277.6 8.7 %all-gather.6.cloned.1.call-done = bf16[32,1,12,2048]{3,0,2,1:T(8,128)(2,1)} async-done(((bf16[16,1,12,2048]{3,0,2,1:T(8,128)(2,1)}), bf16[32,1,12,2048]{3,0,2,1:T(8,128)(2,1)}) %all-gather.6.cloned.1.call-update) | async-done | bytes 1572880 | tf_op jit(solution)/shard_map/all_gather | solution.py:155
  286.3 2.8 reduce.2
  289.2 2.6 copy.76
  291.8 7.1 %all-to-all-start.2 = ((bf16[16,12,2048]{2,1,0:T(8,128)(2,1)}), bf16[16,12,2048]{2,1,0:T(8,128)(2,1)}, u32[]{:S(2)}, u32[]{:S(2)}) async-start(bf16[16,12,2048]{2,1,0:T(8,128)(2,1)} %copy.76), calls=%async_computation.3 | async-start | bytes 2097152 | tf_op jit(solution)/shard_map/all_to_all | solution.py:157
  298.9 0.1 reduce_sum.82
  299.0 0.1 copy.73
  299.1 0.7 copy.77
  299.7 25.1 %all-to-all-done.2 = bf16[16,12,2048]{2,1,0:T(8,128)(2,1)} async-done(((bf16[16,12,2048]{2,1,0:T(8,128)(2,1)}), bf16[16,12,2048]{2,1,0:T(8,128)(2,1)}, u32[]{:S(2)}, u32[]{:S(2)}) %all-to-all-start.2) | async-done | bytes 786464 | tf_op jit(solution)/shard_map/all_to_all | solution.py:157
  324.9 2.1 reshape.170
  327.0 1.5 fusion.21
  328.5 0.7 fusion.44
  (36 shorter events, 0.1 us)
Async XLA Ops:
  7.2 265.2 %copy-start = (bf16[1,704,2048]{2,1,0:T(8,128)(2,1)S(1)}, bf16[1,704,2048]{2,1,0:T(8,128)(2,1)}, u32[]{:S(2)}) copy-start(bf16[1,704,2048]{2,1,0:T(8,128)(2,1)} %param.39) | copy-start | bytes 8650756
  10.1 13.8 %all-to-all-start = ((bf16[32,16,128]{2,0,1:T(8,128)(2,1)}), bf16[32,16,128]{2,0,1:T(8,128)(2,1)S(1)}, u32[]{:S(2)}, u32[]{:S(2)}) async-start(bf16[32,16,128]{2,0,1:T(8,128)(2,1)} %copy_bitcast_fusion), calls=%async_computation | async-start | bytes 262144 | tf_op jit(solution)/shard_map/all_to_all | solution.py:82
  17.3 135.7 %reduce-scatter.2.cloned.1.call-start = ((), (), s32[]{:S(2)}) async-start(), calls=%async_computation.4 | async-start | bytes 2506752 | tf_op jit(solution)/shard_map/reduce_scatter | solution.py:84
  18.9 7.6 %copy-start.13 = (f32[32,4]{0,1:T(4,128)S(1)}, f32[32,4]{0,1:T(4,128)}, u32[]{:S(2)}) copy-start(f32[32,4]{0,1:T(4,128)} %param.35) | copy-start | bytes 1540
  18.9 7.7 %copy-start.7 = (s32[32,3]{0,1:T(4,128)S(1)}, s32[32,3]{0,1:T(4,128)}, u32[]{:S(2)}) copy-start(s32[32,3]{0,1:T(4,128)} %param.40) | copy-start | bytes 1156
  23.9 130.5 %copy-start.10 = (f32[4]{0:T(128)S(1)}, f32[4]{0:T(128)}, u32[]{:S(2)}) copy-start(f32[4]{0:T(128)} %param.30) | copy-start | bytes 52
  23.9 130.5 %copy-start.15 = (f32[4]{0:T(128)S(1)}, f32[4]{0:T(128)}, u32[]{:S(2)}) copy-start(f32[4]{0:T(128)} %param.29) | copy-start | bytes 52
  23.9 132.2 %copy-start.5 = (f32[32,4,64]{2,1,0:T(4,128)S(1)}, f32[32,4,64]{2,1,0:T(4,128)}, u32[]{:S(2)}) copy-start(f32[32,4,64]{2,1,0:T(4,128)} %param.34) | copy-start | bytes 98308
  25.8 179.9 %all-gather.4.cloned.1.call-start = ((), (), s32[]{:S(2)}) async-start(), calls=%async_computation.5 | async-start | bytes 1114112 | tf_op jit(solution)/shard_map/all_gather | solution.py:116
  26.5 200.0 %all-reduce.2.cloned.1.call-start = ((), (), s32[]{:S(2)}) async-start(), calls=%async_computation.6 | async-start | bytes 262144 | tf_op jit(solution)/shard_map/psum | solution.py:119
  27.3 180.6 %copy-start.11 = (s32[96]{0:T(128)}, s32[96]{0:T(128)S(1)}, u32[]{:S(2)}) copy-start(s32[96]{0:T(128)S(1)} %select_reduce_fusion) | copy-start | bytes 1156
  160.7 2.0 copy-start.1
  162.7 43.0 %copy-start.14 = (f32[256]{0:T(256)S(1)}, f32[256]{0:T(256)}, u32[]{:S(2)}) copy-start(f32[256]{0:T(256)} %param.31) | copy-start | bytes 3076
  162.7 63.8 %copy-start.2 = (bf16[32,2048]{1,0:T(8,128)(2,1)S(1)}, bf16[32,2048]{1,0:T(8,128)(2,1)}, u32[]{:S(2)}) copy-start(bf16[32,2048]{1,0:T(8,128)(2,1)} %param.21) | copy-start | bytes 393220
  162.7 64.9 %copy-start.6 = (f32[2048]{0:T(1024)S(1)}, f32[2048]{0:T(1024)}, u32[]{:S(2)}) copy-start(f32[2048]{0:T(1024)} %param.36) | copy-start | bytes 24580
  207.9 78.4 %all-gather.6.cloned.1.call-start = ((), (), s32[]{:S(2)}) async-start(), calls=%async_computation.7 | async-start | bytes 2359296 | tf_op jit(solution)/shard_map/all_gather | solution.py:155
  267.6 1.0 copy-start.4
  286.3 12.6 %copy-start.12 = (s32[96]{0:T(128)S(1)}, s32[96]{0:T(128)}, u32[]{:S(2)}) copy-start(s32[96]{0:T(128)} %copy-done.11) | copy-start | bytes 1156
  286.3 12.8 %copy-start.8 = (s32[32,3]{0,1:T(4,128)S(1)}, s32[32,3]{0,1:T(4,128)}, u32[]{:S(2)}) copy-start(s32[32,3]{0,1:T(4,128)} %param.40) | copy-start | bytes 1156
  289.2 37.8 %copy-start.9 = (f32[32,3]{0,1:T(4,128)S(1)}, f32[32,3]{0,1:T(4,128)}, u32[]{:S(2)}) copy-start(f32[32,3]{0,1:T(4,128)} %param.41) | copy-start | bytes 1156
  291.8 36.7 %copy-start.3 = (bf16[32,2048]{1,0:T(8,128)(2,1)S(1)}, bf16[32,2048]{1,0:T(8,128)(2,1)}, u32[]{:S(2)}) copy-start(bf16[32,2048]{1,0:T(8,128)(2,1)} %all-reduce.2.cloned.1.call-done) | copy-start | bytes 393220
  291.8 33.1 %all-to-all-start.2 = ((bf16[16,12,2048]{2,1,0:T(8,128)(2,1)}), bf16[16,12,2048]{2,1,0:T(8,128)(2,1)}, u32[]{:S(2)}, u32[]{:S(2)}) async-start(bf16[16,12,2048]{2,1,0:T(8,128)(2,1)} %copy.76), calls=%async_computation.3 | async-start | bytes 2097152 | tf_op jit(solution)/shard_map/all_to_all | solution.py:157
Sparse Core Ops, SparseCore 0:
  25.9 127.0 reduce-scatter.1
  155.7 49.9 all-gather.3
  208.6 17.9 all-reduce.1
  277.7 8.5 all-gather.5
